TPU v7x, 32 devices: a whole 2x2x4 slice. The times are simulated.
32 devices in a mesh: sp: 8 (over z, y), tp: 4 (over x, core).
Axes of the slice: x: 2, y: 2, z: 4, core: 2. Of those that a mesh axis runs over, the one named last changes fastest.
Arguments:
- resid: bfloat16 [8192, 2048], P(('sp', 'tp')), may hold values from -6 to 6
- query_nope: bfloat16 [8192, 2048], P('sp', 'tp'), may hold values from -18 to 18
- query_rope: bfloat16 [8192, 1024], P('sp', 'tp'), may hold values from -300 to 300
- latent: bfloat16 [8192, 256], P('sp'), may hold values from -6 to 6
- key_rope: bfloat16 [8192, 64], P('sp'), may hold values from -6 to 6
- latent_gain: float32 [256], replicated, may hold values from 0.1 to 1.9
- w_key: bfloat16 [256, 2048], P(None, 'tp'), may hold values from -0.375 to 0.375
- w_value: bfloat16 [256, 2048], P(None, 'tp'), may hold values from -0.375 to 0.375
- w_out: bfloat16 [2048, 2048], P('tp'), may hold values from -0.125 to 0.125
- mix_gain: float32 [2048], replicated, may hold values from 0.1 to 1.9
- w_gate: bfloat16 [2048, 5632], P('sp', 'tp'), may hold values from -0.125 to 0.125
- w_up: bfloat16 [2048, 5632], P('sp', 'tp'), may hold values from -0.125 to 0.125
- w_down: bfloat16 [2048, 5632], P('sp', 'tp'), may hold values from -0.078125 to 0.078125
Outputs:
- layer_out: bfloat16 [8192, 2048], P(('sp', 'tp'))
All inputs are finite; a program needn't handle non-finite values.
Results may differ from a plain program's by a relative error of at most 0.0095.
Values may be sent and summed in bfloat16 or wider, within the bound.
A program may use at most 128 MiB of HBM per device.

v0:
```python
import jax
import jax.numpy as jnp
from jax import lax
from jax.sharding import PartitionSpec as P

NOPE = 128
ROPE = 64
VDIM = 128


norm_eps = 1e-06
masked_score = -1e30
theta_base = 10000.0


def rotate(values_in, angle):
    half_width = values_in.shape[-1] // 2
    front_half = values_in[..., :half_width]
    back_half = values_in[..., half_width:]
    cosine = jnp.cos(angle)
    sine_part = jnp.sin(angle)
    return jnp.concatenate(
        [front_half * cosine - back_half * sine_part, back_half * cosine + front_half * sine_part],
        axis=-1,
    )


def angles(positions, full_width):
    half_width = full_width // 2
    frequency = theta_base ** (-2.0 * jnp.arange(half_width).astype(jnp.float32) / full_width)
    return positions[:, None] * frequency[None, :]


def rms_scale(values_in, gain):
    return (
        values_in
        * lax.rsqrt(jnp.mean(values_in * values_in, axis=-1, keepdims=True) + norm_eps)
        * gain
    )


def attend(fold_state, queries, key_block, value_block, rope_block, block_start):
    nope_query, rope_query, query_rows = queries
    running_max, weight_sum, accumulated = fold_state
    key_rows = block_start + jnp.arange(key_block.shape[0], dtype=jnp.int32)
    causal = key_rows[None, :] <= query_rows[:, None]
    scores = jnp.einsum("qhd,khd->hqk", nope_query, key_block, preferred_element_type=jnp.float32)
    scores = scores + jnp.einsum(
        "qhr,kr->hqk", rope_query, rope_block, preferred_element_type=jnp.float32
    )
    scores = jnp.where(causal[None], scores * (NOPE + ROPE) ** (-0.5), masked_score)
    new_max = jnp.maximum(running_max, jnp.max(scores, axis=-1))
    weights = jnp.where(causal[None], jnp.exp(scores - new_max[..., None]), 0.0)
    factor = jnp.exp(running_max - new_max)
    weight_sum = weight_sum * factor + jnp.sum(weights, axis=-1)
    accumulated = accumulated * factor[..., None] + jnp.einsum(
        "hqk,khd->hqd",
        weights.astype(jnp.bfloat16),
        value_block,
        preferred_element_type=jnp.float32,
    )
    return (new_max, weight_sum, accumulated)


def over_blocks(fold_state, arrays, last_query, step_fn, row_count):
    piece_rows = arrays[0].shape[0]
    candidates = [
        row_count * multiple
        for multiple in (4, 2, 1)
        if piece_rows % (row_count * multiple) == 0 and row_count * multiple <= 2048
    ]
    block_rows = candidates[0]
    block_count = piece_rows // block_rows
    stacked = tuple(
        (member.reshape((block_count, block_rows) + member.shape[1:]) for member in arrays)
    )

    def advance(state_in, indexed):
        block_index, blocks_now = indexed
        block_start = block_index * block_rows

        def compute(state_now):
            return step_fn(state_now, blocks_now, block_start)

        def unchanged(state_now):
            return state_now

        return (lax.cond(block_start <= last_query, compute, unchanged, state_in), None)

    result, ignored = lax.scan(
        advance, fold_state, (jnp.arange(block_count, dtype=jnp.int32), stacked)
    )
    return result


def on_device(
    resid,
    query_nope,
    query_rope,
    latent,
    key_rope,
    latent_gain,
    w_key,
    w_value,
    w_out,
    mix_gain,
    w_gate,
    w_up,
    w_down,
):
    row_count = query_nope.shape[0]
    head_count = query_nope.shape[1] // NOPE
    first_row = lax.axis_index("sp") * row_count
    query_rows = first_row + jnp.arange(row_count, dtype=jnp.int32)
    angle = angles(query_rows.astype(jnp.float32), ROPE)
    nope_query = query_nope.reshape(row_count, head_count, NOPE)
    rope_query = rotate(
        query_rope.astype(jnp.float32).reshape(row_count, head_count, ROPE), angle[:, None, :]
    ).astype(jnp.bfloat16)
    latent_normed = rms_scale(latent.astype(jnp.float32), latent_gain).astype(jnp.bfloat16)
    key_rotated = rotate(key_rope.astype(jnp.float32), angle).astype(jnp.bfloat16)
    queries = (nope_query, rope_query, query_rows)
    last_query = first_row + row_count - 1
    initial = (
        jnp.full((head_count, row_count), masked_score, jnp.float32),
        jnp.zeros((head_count, row_count), jnp.float32),
        jnp.zeros((head_count, row_count, VDIM), jnp.float32),
    )
    gate_full, up_full, down_full = (
        lax.all_gather(w_gate, "sp", axis=0, tiled=True),
        lax.all_gather(w_up, "sp", axis=0, tiled=True),
        lax.all_gather(w_down, "sp", axis=0, tiled=True),
    )

    def expand_block(state_now, blocks_now, block_start):
        latent_block, rope_block = blocks_now
        key_block = jnp.dot(latent_block, w_key, preferred_element_type=jnp.float32).astype(
            jnp.bfloat16
        )
        value_block = jnp.dot(latent_block, w_value, preferred_element_type=jnp.float32).astype(
            jnp.bfloat16
        )
        return attend(
            state_now,
            queries,
            key_block.reshape(-1, head_count, NOPE),
            value_block.reshape(-1, head_count, VDIM),
            rope_block,
            block_start,
        )

    final_state = over_blocks(
        initial,
        (
            lax.all_gather(latent_normed, "sp", axis=0, tiled=True),
            lax.all_gather(key_rotated, "sp", axis=0, tiled=True),
        ),
        last_query,
        expand_block,
        row_count,
    )
    head_out = (final_state[2] / final_state[1][..., None]).astype(jnp.bfloat16)
    out_heads = w_out.reshape(head_count, VDIM, w_out.shape[1])
    part_rows = head_out
    head_term = jnp.einsum("hqv,hvd->qd", part_rows, out_heads, preferred_element_type=jnp.float32)
    attention_proj = lax.psum_scatter(
        lax.optimization_barrier(head_term.astype(jnp.bfloat16))
        .astype(jnp.float32)
        .astype(jnp.bfloat16),
        "tp",
        scatter_dimension=0,
        tiled=True,
    ).astype(jnp.float32)
    stream = resid.astype(jnp.float32) + attention_proj
    normed = rms_scale(stream, mix_gain).astype(jnp.bfloat16)
    row_piece = lax.all_gather(normed, "tp", axis=0, tiled=True)
    gate_value = jnp.dot(row_piece, gate_full, preferred_element_type=jnp.float32)
    upward = jnp.dot(row_piece, up_full, preferred_element_type=jnp.float32)
    hidden = (jax.nn.silu(gate_value) * upward).astype(jnp.bfloat16)
    part_rows = hidden
    down_term = lax.dot_general(
        part_rows, down_full, (((1,), (1,)), ((), ())), preferred_element_type=jnp.float32
    )
    mixer_out = lax.psum_scatter(
        lax.optimization_barrier(down_term.astype(jnp.bfloat16))
        .astype(jnp.float32)
        .astype(jnp.bfloat16),
        "tp",
        scatter_dimension=0,
        tiled=True,
    ).astype(jnp.float32)
    return (stream + 0.5 * mixer_out).astype(jnp.bfloat16)


def solution(mesh):
    return jax.shard_map(
        on_device,
        mesh=mesh,
        in_specs=(
            P(("sp", "tp"), None),
            P("sp", "tp"),
            P("sp", "tp"),
            P("sp", None),
            P("sp", None),
            P(),
            P(None, "tp"),
            P(None, "tp"),
            P("tp", None),
            P(),
            P("sp", "tp"),
            P("sp", "tp"),
            P("sp", "tp"),
        ),
        out_specs=P(("sp", "tp"), None),
        check_vma=False,
    )
```

profile of v0, /device:TPU:0, one launch (start us, length us, event | category | flops | bytes accessed | tf_op | source)
XLA Modules:
  0.0 855.5 jit_solution(10297096689467318727)
XLA Ops:
  6.6 1.1 convert_element_type.78
  7.7 1.2 multiply_cosine_fusion
  8.9 0.7 pad_maximum_fusion.1
  9.6 0.0 all-gather.7.cloned.1.call-start
  9.6 1.3 fusion.21
  10.9 2.0 fusion.23
  13.0 0.0 reduce-scatter.3.cloned.1.call-start
  13.0 2.2 copy.22
  15.2 1.3 copy.21
  16.5 1.7 copy.23
  18.2 1.4 subtract_convert_fusion
  19.6 0.8 pad_maximum_fusion
  20.4 32.3 %all-gather.9.cloned.1.call-done = bf16[8192,64]{0,1:T(8,128)(2,1)} async-done(((bf16[1024,64]{0,1:T(8,128)(2,1)}), bf16[8192,64]{0,1:T(8,128)(2,1)}) %all-gather.9.cloned.1.call-update) | async-done | bytes 1048592 | tf_op jit(solution)/shard_map/all_gather | solution.py:156
  52.7 2.3 copy.30
  55.0 71.4 %all-gather.7.cloned.1.call-done = bf16[8192,256]{1,0:T(8,128)(2,1)} async-done(((bf16[1024,256]{1,0:T(8,128)(2,1)}), bf16[8192,256]{1,0:T(8,128)(2,1)}) %all-gather.7.cloned.1.call-update) | async-done | bytes 4194320 | tf_op jit(solution)/shard_map/all_gather | solution.py:155
  126.4 1.4 broadcast_in_dim.50
  127.8 76.5 %while.15 = (s32[]{:T(128)}, f32[4,1024]{1,0:T(4,128)S(1)}, f32[4,1024]{1,0:T(4,128)S(1)}, f32[4,1024,128]{2,1,0:T(8,128)}, s32[4]{0:T(128)S(1)}, /*index=5*/s32...) while((s32[]{:T(128)}, f32[4,1024]{1,0:T(4,128)S(1)}, ...), condition=%wide.region_6.7_spmd.clone, body=%wide.region_1.6_spmd.clone.sunk | while | flops 6531591168 | bytes 213419984 | solution.py:90
  127.8 0.7 dynamic_slice.38
  129.2 71.1 %conditional.3 = ((f32[4,1024]{1,0:T(4,128)S(1)}, f32[4,1024]{1,0:T(4,128)S(1)}, f32[4,1024,128]{2,1,0:T(8,128)})) conditional(s32[]{:T(128)} %convert_element_type.134, (f32[4,1024]{1,0:T(4,128)S(1)}, f32[4,1024]{1,0:T(4,128)S(1)}, f32[4,1024,128]{2,1,0:T(8,128)}) %tuple.44, (s32[]{:T(128)}, s32[]{:T(128)}, bf16[4,2048,256]{2,1,0:T(8,128)(2,1)}, ...), branch_computations={%region_2.2_spmd, %region_3.5_spmd} | conditional | flops 6531591168 | bytes 213415584 | solution.py:88
  129.2 2.0 convolution_convert_fusion.1
  131.2 13.2 %fusion.26 = f32[4,2048,1024]{2,1,0:T(8,128)} fusion(bf16[2048,4,128]{0,2,1:T(8,128)(2,1)S(1)} %bitcast.56, bf16[1024,4,128]{2,0,1:T(8,128)(2,1)S(1)} %get-tuple-element.152), kind=kOutput, calls=%fused_computation.55 | convolution fusion | flops 2147483648 | bytes 36700160 | tf_op jit(solution)/shard_map/while/body/eval_jaxpr/cond/branch_1_fun/qhd,khd->hqk/dot_general | solution.py:47
  144.3 1.3 broadcast_compare_fusion
  145.7 22.8 %fusion.25 = (f32[4,1024]{1,0:T(4,128)S(1)}, f32[4,1024,2048]{1,2,0:T(8,128)}) fusion(bf16[1024,4,64]{0,2,1:T(8,128)(2,1)S(1)} %copy-done.1, bf16[4,2048,64]{1,2,0:T(8,128)(2,1)} %get-tuple-element.153, s32[]{:T(128)} %get-tuple-element.150, f32[4,2048,1024]{2,1,0:T(8,128)} %fusion.26, pred[1024,2048]{0,1:T(8,128)(4,1)S(1)} %broadcast_compare_fusion), kind=kOutput, calls=%fused_computation.54 | convolution fusion | flops 1107292160 | bytes 70009344 | tf_op jit(solution)/shard_map/while/body/eval_jaxpr/cond/branch_1_fun/qhr,kr->hqk/dot_general | solution.py:48
  168.5 14.0 %fusion.5 = f32[4,1024]{1,0:T(4,128)S(1)} fusion(f32[4,1024,2048]{1,2,0:T(8,128)} %get-tuple-element.256, f32[4,1024]{1,0:T(4,128)S(1)} %max.4, pred[1024,2048]{0,1:T(8,128)(4,1)S(1)} %broadcast_compare_fusion), kind=kLoop, calls=%fused_computation.6 | loop fusion | flops 25161728 | bytes 35684352 | tf_op jit(solution)/shard_map/while/body/eval_jaxpr/cond/branch_1_fun/reduce_sum | solution.py:55
  182.5 2.0 convolution_convert_fusion
  184.5 14.4 %multiply_add_fusion = f32[4,1024,128]{2,1,0:T(8,128)S(1)} fusion(f32[4,1024,128]{2,1,0:T(8,128)S(1)} %copy-done.5, bf16[2048,4,128]{0,2,1:T(8,128)(2,1)S(1)} %bitcast.57, f32[4,1024,2048]{1,2,0:T(8,128)} %get-tuple-element.256, f32[4,1024]{1,0:T(4,128)S(1)} %max.4, pred[1024,2048]{0,1:T(8,128)(4,1)S(1)} %broadcast_compare_fusion, ...), kind=kOutput, calls=%fused_computation.12 | convolution fusion | flops 2173698048 | bytes 41975808 | tf_op jit(solution)/shard_map/while/body/eval_jaxpr/cond/branch_1_fun/hqk,khd->hqd/dot_general | solution.py:56
  199.0 1.3 copy-done.6
  200.3 0.7 dynamic_slice.38
  201.6 0.7 dynamic_slice.38
  203.0 0.7 dynamic_slice.38
  204.3 5.7 bitcast_convert_fusion
  210.0 0.2 all-gather.13.cloned.1.call-start
  210.3 0.3 all-gather.13.cloned.1.call-update
  210.6 0.0 all-gather.11.cloned.1.call-start
  210.7 255.8 %reduce-scatter.3.cloned.1.call-done = bf16[256,2048]{1,0:T(8,128)(2,1)} async-done(((bf16[1024,2048]{1,0:T(8,128)(2,1)}), bf16[256,2048]{1,0:T(8,128)(2,1)}) %reduce-scatter.3.cloned.1.call-update) | async-done | bytes 1048592 | tf_op jit(solution)/shard_map/reduce_scatter | solution.py:166
  466.5 1.6 multiply_reduce_fusion
  468.2 2.6 multiply_convert_fusion.1
  470.8 0.0 all-gather.15.cloned.1.call-start
  470.8 0.5 all-gather.15.cloned.1.call-update
  471.4 0.7 all-gather.17.cloned.1.call-update
  472.1 88.7 %all-gather.13.cloned.1.call-done = bf16[2048,1408]{1,0:T(8,128)(2,1)} async-done(((bf16[256,1408]{1,0:T(8,128)(2,1)}), bf16[2048,1408]{1,0:T(8,128)(2,1)}) %all-gather.13.cloned.1.call-update) | async-done | bytes 5767184 | tf_op jit(solution)/shard_map/all_gather | solution.py:130
  560.9 34.1 %all-gather.11.cloned.1.call-done = bf16[1024,2048]{1,0:T(8,128)(2,1)} async-done(((bf16[256,2048]{1,0:T(8,128)(2,1)}), bf16[1024,2048]{1,0:T(8,128)(2,1)}) %all-gather.11.cloned.1.call-update) | async-done | bytes 4194320 | tf_op jit(solution)/shard_map/all_gather | solution.py:176
  595.0 11.7 %fusion.27 = f32[1024,1408]{1,0:T(8,128)} fusion(bf16[1024,2048]{1,0:T(8,128)(2,1)} %all-gather.11.cloned.1.call-done, bf16[2048,1408]{1,0:T(8,128)(2,1)} %all-gather.13.cloned.1.call-done), kind=kOutput, calls=%fused_computation.56 | convolution fusion | flops 5905580032 | bytes 15728640 | tf_op jit(solution)/shard_map/dot_general | solution.py:177
  606.6 82.7 %all-gather.15.cloned.1.call-done = bf16[2048,1408]{1,0:T(8,128)(2,1)} async-done(((bf16[256,1408]{1,0:T(8,128)(2,1)}), bf16[2048,1408]{1,0:T(8,128)(2,1)}) %all-gather.15.cloned.1.call-update) | async-done | bytes 5767184 | tf_op jit(solution)/shard_map/all_gather | solution.py:131
  689.3 92.7 %all-gather.17.cloned.1.call-done = bf16[2048,1408]{1,0:T(8,128)(2,1)} async-done(((bf16[256,1408]{1,0:T(8,128)(2,1)}), bf16[2048,1408]{1,0:T(8,128)(2,1)}) %all-gather.17.cloned.1.call-update) | async-done | bytes 5767184 | tf_op jit(solution)/shard_map/all_gather | solution.py:132
  782.0 20.6 %convolution_convert_fusion.2 = bf16[1024,2048]{1,0:T(8,128)(2,1)} fusion(bf16[2048,1408]{1,0:T(8,128)(2,1)} %all-gather.17.cloned.1.call-done, f32[1024,1408]{1,0:T(8,128)} %fusion.27, bf16[1024,2048]{1,0:T(8,128)(2,1)} %all-gather.11.cloned.1.call-done, bf16[2048,1408]{1,0:T(8,128)(2,1)} %all-gather.15.cloned.1.call-done), kind=kOutput, calls=%fused_computation.29 | convolution fusion | flops 11821907968 | bytes 25690112 | tf_op jit(solution)/shard_map/dot_general | solution.py:181
  802.6 42.9 %reduce-scatter.5.cloned.1.call-done = bf16[256,2048]{1,0:T(8,128)(2,1)} async-done(((bf16[1024,2048]{1,0:T(8,128)(2,1)}), bf16[256,2048]{1,0:T(8,128)(2,1)}) %reduce-scatter.5.cloned.1.call-update) | async-done | bytes 1048592 | tf_op jit(solution)/shard_map/reduce_scatter | solution.py:184
  845.6 3.1 add_convert_fusion
  (44 shorter events, 0.3 us)
Async XLA Ops:
  6.5 197.8 %copy-start = (bf16[512,2048]{1,0:T(8,128)(2,1)S(1)}, bf16[512,2048]{1,0:T(8,128)(2,1)}, u32[]{:S(2)}) copy-start(bf16[512,2048]{1,0:T(8,128)(2,1)} %param.25) | copy-start | bytes 6291460
  6.5 8.7 %copy-start.7 = (bf16[1024,512]{1,0:T(8,128)(2,1)S(1)}, bf16[1024,512]{1,0:T(8,128)(2,1)}, u32[]{:S(2)}) copy-start(bf16[1024,512]{1,0:T(8,128)(2,1)} %param.18) | copy-start | bytes 3145732
  6.5 46.2 %all-gather.9.cloned.1.call-start = ((), (), s32[]{:S(2)}) async-start(), calls=%async_computation.3 | async-start | bytes 1179648 | tf_op jit(solution)/shard_map/all_gather | solution.py:156
  9.6 116.8 %all-gather.7.cloned.1.call-start = ((), (), s32[]{:S(2)}) async-start(), calls=%async_computation.2 | async-start | bytes 4718592 | tf_op jit(solution)/shard_map/all_gather | solution.py:155
  13.0 453.5 %reduce-scatter.3.cloned.1.call-start = ((), (), s32[]{:S(2)}) async-start(), calls=%async_computation.4 | async-start | bytes 5242880 | tf_op jit(solution)/shard_map/reduce_scatter | solution.py:166
  16.5 111.3 %copy-start.3 = (bf16[256,512]{1,0:T(8,128)(2,1)S(1)}, bf16[256,512]{1,0:T(8,128)(2,1)}, u32[]{:S(2)}) copy-start(bf16[256,512]{1,0:T(8,128)(2,1)} %param.23) | copy-start | bytes 786436
  131.2 14.5 %copy-start.1 = (bf16[1024,4,64]{0,2,1:T(8,128)(2,1)S(1)}, bf16[1024,4,64]{0,2,1:T(8,128)(2,1)}, u32[]{:S(2)}) copy-start(bf16[1024,4,64]{0,2,1:T(8,128)(2,1)} %get-tuple-element.154) | copy-start | bytes 1572868 | tf_op jit(solution)/shard_map/while/body/eval_jaxpr/cond
  168.5 14.0 %copy-start.4 = (bf16[256,512]{1,0:T(8,128)(2,1)S(1)}, bf16[256,512]{1,0:T(8,128)(2,1)}, u32[]{:S(2)}) copy-start(bf16[256,512]{1,0:T(8,128)(2,1)} %get-tuple-element.157) | copy-start | bytes 786436 | tf_op jit(solution)/shard_map/while/body/eval_jaxpr/cond
  168.5 16.0 %copy-start.5 = (f32[4,1024,128]{2,1,0:T(8,128)S(1)}, f32[4,1024,128]{2,1,0:T(8,128)}, u32[]{:S(2)}) copy-start(f32[4,1024,128]{2,1,0:T(8,128)} %get-tuple-element.156) | copy-start | bytes 6291460 | tf_op jit(solution)/shard_map/while/body/eval_jaxpr/cond
  199.0 1.3 copy-start.6
  210.0 256.5 %copy-start.2 = (bf16[256,2048]{1,0:T(8,128)(2,1)S(1)}, bf16[256,2048]{1,0:T(8,128)(2,1)}, u32[]{:S(2)}) copy-start(bf16[256,2048]{1,0:T(8,128)(2,1)} %param.17) | copy-start | bytes 3145732
  210.0 258.1 %copy-start.8 = (f32[2048]{0:T(1024)S(1)}, f32[2048]{0:T(1024)}, u32[]{:S(2)}) copy-start(f32[2048]{0:T(1024)} %param.26) | copy-start | bytes 24580
  210.0 350.8 %all-gather.13.cloned.1.call-start = ((), (), s32[]{:S(2)}) async-start(), calls=%async_computation.6 | async-start | bytes 6488064 | tf_op jit(solution)/shard_map/all_gather | solution.py:130
  210.6 384.3 %all-gather.11.cloned.1.call-start = ((), (), s32[]{:S(2)}) async-start(), calls=%async_computation.5 | async-start | bytes 5242880 | tf_op jit(solution)/shard_map/all_gather | solution.py:176
  470.8 218.6 %all-gather.15.cloned.1.call-start = ((), (), s32[]{:S(2)}) async-start(), calls=%async_computation.7 | async-start | bytes 6488064 | tf_op jit(solution)/shard_map/all_gather | solution.py:131
  471.4 310.7 %all-gather.17.cloned.1.call-start = ((), (), s32[]{:S(2)}) async-start(), calls=%async_computation.8 | async-start | bytes 6488064 | tf_op jit(solution)/shard_map/all_gather | solution.py:132
  472.1 373.5 %reduce-scatter.5.cloned.1.call-start = ((), (), s32[]{:S(2)}) async-start(), calls=%async_computation.9 | async-start | bytes 5242880 | tf_op jit(solution)/shard_map/reduce_scatter | solution.py:184
Sparse Core Ops, SparseCore 0:
  9.7 42.9 all-gather.8
  54.8 71.4 all-gather.6
  210.2 256.2 reduce-scatter.2
  468.5 92.2 all-gather.12
  562.3 32.6 all-gather.10
  597.0 92.3 all-gather.14
  691.5 90.4 all-gather.16
  802.8 42.7 reduce-scatter.4
where the time goes:
time: 857 us; the launch traced here: 855 us
  waiting for transfers between devices  702 us (82%)
  matrix products  92.3 us (11%)
  other arithmetic  31.1 us (4%)
  between operations  13.6 us (2%)
  local copies, waits for them, and re-layouts  12.9 us (2%)
    reduce_scatter x1, waiting for transfers between devices, on_device(): lax.psum_scatter(lax.optimization_barrier(head_term.astype(jnp.bfloat16))...  256 us
    all_gather x1, waiting for transfers between devices, on_device(): lax.all_gather(w_down, 'sp', axis=0, tiled=True)  92.7 us
    all_gather x1, waiting for transfers between devices, on_device(): lax.all_gather(w_gate, 'sp', axis=0, tiled=True)  88.7 us
    all_gather x1, waiting for transfers between devices, on_device(): lax.all_gather(w_up, 'sp', axis=0, tiled=True)  82.7 us
    all_gather x1, waiting for transfers between devices, on_device(): lax.all_gather(latent_normed, 'sp', axis=0, tiled=True)  71.4 us
    reduce_scatter x1, waiting for transfers between devices, on_device(): lax.psum_scatter(lax.optimization_barrier(down_term.astype(jnp.bfloat16))...  42.9 us
    all_gather x1, waiting for transfers between devices, on_device(): row_piece = lax.all_gather(normed, 'tp', axis=0, tiled=True)  34.1 us
    all_gather x1, waiting for transfers between devices, on_device(): lax.all_gather(key_rotated, 'sp', axis=0, tiled=True)  32.3 us
  transfers between devices with their start and end apart: 8, of which 8 were waited for; matrix products, arithmetic and copies ran while one was open for 3% of the time, Pallas kernels for 0%

commit v1 on v0

v1 whole, which is shorter than its diff:
```python
import functools

import jax
import jax.numpy as jnp
from jax import lax
from jax.experimental import pallas as pl
from jax.experimental.pallas import tpu as pltpu
from jax.sharding import PartitionSpec as P

NOPE = 128
ROPE = 64
VDIM = 128
PAD = 64


norm_eps = 1e-06
masked_score = -1e30
theta_base = 10000.0
LOG2E = 1.4426950408889634
COLS = (((1,), (1,)), ((), ()))


def rotate(values_in, angle):
    half_width = values_in.shape[-1] // 2
    front_half = values_in[..., :half_width]
    back_half = values_in[..., half_width:]
    cosine = jnp.cos(angle)
    sine_part = jnp.sin(angle)
    return jnp.concatenate(
        [front_half * cosine - back_half * sine_part, back_half * cosine + front_half * sine_part],
        axis=-1,
    )


def angles(positions, full_width):
    half_width = full_width // 2
    frequency = theta_base ** (-2.0 * jnp.arange(half_width).astype(jnp.float32) / full_width)
    return positions[:, None] * frequency[None, :]


def rms_scale(values_in, gain):
    return (
        values_in
        * lax.rsqrt(jnp.mean(values_in * values_in, axis=-1, keepdims=True) + norm_eps)
        * gain
    )


def attention_kernel(tile, q_ref, lat_ref, wk_ref, wv_ref, o_ref, k_ref, v_ref, m_ref, acc_ref):
    step = pl.program_id(0)
    me = lax.axis_index("sp")
    heads, rows, width = q_ref.shape
    rank = wk_ref.shape[1]
    tiles = rows // tile
    scale = (NOPE + ROPE) ** (-0.5) * LOG2E

    @pl.when(step == 0)
    def _():
        m_ref[...] = jnp.full_like(m_ref, masked_score)
        acc_ref[...] = jnp.zeros_like(acc_ref)

    def project(h):
        block = lat_ref[:, :rank]
        keys = jnp.dot(block, wk_ref[h], preferred_element_type=jnp.float32)
        k_ref[:, :NOPE] = keys.astype(jnp.bfloat16)
        k_ref[:, NOPE:] = lat_ref[:, rank:]
        values = jnp.dot(block, wv_ref[h], preferred_element_type=jnp.float32)
        v_ref[:, :VDIM] = values.astype(jnp.bfloat16)
        v_ref[:, VDIM:] = jnp.ones((rows, width - VDIM), jnp.bfloat16)

    def fold(h, t, keys, diagonal):
        span = pl.ds(t * tile, tile)
        scores = lax.dot_general(
            q_ref[h, span, :], k_ref[:keys, :], COLS, preferred_element_type=jnp.float32
        )
        if diagonal:
            row = t * tile + lax.broadcasted_iota(jnp.int32, scores.shape, 0)
            col = lax.broadcasted_iota(jnp.int32, scores.shape, 1)
            scores = jnp.where(col <= row, scores, masked_score)
        old = m_ref[h, span, :]
        top = jnp.maximum(old, jnp.max(scores, axis=1, keepdims=True))
        weights = jnp.exp2((scores - top[:, :1]) * scale)
        factor = jnp.exp2((old - top) * scale)
        mixed = jnp.dot(
            weights.astype(jnp.bfloat16), v_ref[:keys, :], preferred_element_type=jnp.float32
        )
        m_ref[h, span, :] = top
        acc_ref[h, span, :] = acc_ref[h, span, :] * factor[:, :1] + mixed

    @pl.when(step < me)
    def _():
        def one_head(h, carry):
            project(h)
            for t in range(tiles):
                fold(h, t, rows, False)
            return carry

        lax.fori_loop(0, heads, one_head, 0)

    @pl.when(step == me)
    def _():
        def one_head(h, carry):
            project(h)
            for t in range(tiles):
                fold(h, t, (t + 1) * tile, True)
            done = acc_ref[h]
            out = done[:, :VDIM] / done[:, VDIM : 2 * VDIM]
            o_ref[h] = out.astype(o_ref.dtype)
            return carry

        lax.fori_loop(0, heads, one_head, 0)


def attention(q, lat, wk, wv, steps):
    heads, rows, width = q.shape
    tile = next(size for size in (256, 128, 64, 32, 16, 8) if rows % size == 0)
    whole = lambda shape: pl.BlockSpec(shape, lambda j: (0,) * len(shape))
    flops = 2 * rows * rows * steps * heads * (width + width)
    return pl.pallas_call(
        functools.partial(attention_kernel, tile),
        grid=(steps,),
        out_shape=jax.ShapeDtypeStruct((heads, rows, VDIM), jnp.bfloat16),
        in_specs=[
            whole(q.shape),
            pl.BlockSpec((rows, lat.shape[1]), lambda j: (j, 0)),
            whole(wk.shape),
            whole(wv.shape),
        ],
        out_specs=whole((heads, rows, VDIM)),
        scratch_shapes=[
            pltpu.VMEM((rows, width), jnp.bfloat16),
            pltpu.VMEM((rows, width), jnp.bfloat16),
            pltpu.VMEM((heads, rows, 128), jnp.float32),
            pltpu.VMEM((heads, rows, width), jnp.float32),
        ],
        compiler_params=pltpu.CompilerParams(
            dimension_semantics=("arbitrary",), vmem_limit_bytes=48 * 1024 * 1024
        ),
        cost_estimate=pl.CostEstimate(
            flops=flops, bytes_accessed=2 * rows * 512 * steps, transcendentals=rows * rows * steps
        ),
    )(q, lat, wk, wv)


def on_device(
    n_sp,
    resid,
    query_nope,
    query_rope,
    latent,
    key_rope,
    latent_gain,
    w_key,
    w_value,
    w_out,
    mix_gain,
    w_gate,
    w_up,
    w_down,
):
    row_count = query_nope.shape[0]
    head_count = query_nope.shape[1] // NOPE
    rank = latent.shape[1]
    first_row = lax.axis_index("sp") * row_count
    query_rows = first_row + jnp.arange(row_count, dtype=jnp.int32)
    angle = angles(query_rows.astype(jnp.float32), ROPE)
    latent_normed = rms_scale(latent.astype(jnp.float32), latent_gain).astype(jnp.bfloat16)
    key_rotated = rotate(key_rope.astype(jnp.float32), angle).astype(jnp.bfloat16)
    packed = jnp.concatenate(
        [latent_normed, key_rotated, jnp.zeros((row_count, PAD), jnp.bfloat16)], axis=-1
    )
    latent_all = lax.all_gather(packed, "sp", axis=0, tiled=True)
    gate_full, up_full, down_full = (
        lax.all_gather(w_gate, "sp", axis=0, tiled=True),
        lax.all_gather(w_up, "sp", axis=0, tiled=True),
        lax.all_gather(w_down, "sp", axis=0, tiled=True),
    )
    rope_query = rotate(
        query_rope.astype(jnp.float32).reshape(row_count, head_count, ROPE), angle[:, None, :]
    ).astype(jnp.bfloat16)
    queries = jnp.concatenate(
        [
            query_nope.reshape(row_count, head_count, NOPE),
            rope_query,
            jnp.zeros((row_count, head_count, PAD), jnp.bfloat16),
        ],
        axis=-1,
    ).transpose(1, 0, 2)
    wk = w_key.reshape(rank, head_count, NOPE).transpose(1, 0, 2)
    wv = w_value.reshape(rank, head_count, VDIM).transpose(1, 0, 2)
    head_out = attention(queries, latent_all, wk, wv, n_sp)
    out_heads = w_out.reshape(head_count, VDIM, w_out.shape[1])
    head_term = jnp.einsum("hqv,hvd->qd", head_out, out_heads, preferred_element_type=jnp.float32)
    attention_proj = lax.psum_scatter(
        head_term.astype(jnp.bfloat16), "tp", scatter_dimension=0, tiled=True
    ).astype(jnp.float32)
    stream = resid.astype(jnp.float32) + attention_proj
    normed = rms_scale(stream, mix_gain).astype(jnp.bfloat16)
    row_piece = lax.all_gather(normed, "tp", axis=0, tiled=True)
    gate_value = jnp.dot(row_piece, gate_full, preferred_element_type=jnp.float32)
    upward = jnp.dot(row_piece, up_full, preferred_element_type=jnp.float32)
    hidden = (jax.nn.silu(gate_value) * upward).astype(jnp.bfloat16)
    down_term = lax.dot_general(hidden, down_full, COLS, preferred_element_type=jnp.float32)
    mixer_out = lax.psum_scatter(
        down_term.astype(jnp.bfloat16), "tp", scatter_dimension=0, tiled=True
    ).astype(jnp.float32)
    return (stream + 0.5 * mixer_out).astype(jnp.bfloat16)


def solution(mesh):
    return jax.shard_map(
        functools.partial(on_device, mesh.shape["sp"]),
        mesh=mesh,
        in_specs=(
            P(("sp", "tp"), None),
            P("sp", "tp"),
            P("sp", "tp"),
            P("sp", None),
            P("sp", None),
            P(),
            P(None, "tp"),
            P(None, "tp"),
            P("tp", None),
            P(),
            P("sp", "tp"),
            P("sp", "tp"),
            P("sp", "tp"),
        ),
        out_specs=P(("sp", "tp"), None),
        check_vma=False,
    )
```

time: 857 us -> 630 us (0.74)
  waiting for transfers between devices: 702 us -> 531 us
  matrix products: 92.3 us -> 36.2 us
  Pallas kernels: 0 us -> 15.1 us
  other arithmetic: 31.1 us -> 19.8 us
    reduce_scatter x2, waiting for transfers between devices: 299 us -> 145 us  [the longest x1 103 us: on_device(): lax.psum_scatter(head_term.astype(jnp.bfloat16), 'tp', scatter_dimension=...]
    dot_general x7 -> x2, matrix products: 80.6 us -> 24.5 us  [the longest x1 20.6 us: on_device(): lax.dot_general(hidden, down_full, COLS, preferred_element_type=jnp.float32)]
    all_gather x2 -> x1, waiting for transfers between devices: 104 us -> 85.3 us  [on_device(): latent_all = lax.all_gather(packed, 'sp', axis=0, tiled=True)]
    pallas_call x0 -> x1, Pallas kernels: none -> 15.1 us  [attention(): pl.pallas_call(functools.partial(attention_kernel, tile), grid=(steps,),...]
    reduce_sum x1 -> x0, other arithmetic: 14 us -> none  [attend(): weight_sum = weight_sum * factor + jnp.sum(weights, axis=-1)]
  transfers between devices with their start and end apart: 8 -> 7, of which waited for: 8 -> 7; matrix products, arithmetic and copies ran while one was open for 3% -> 5% of each run, Pallas kernels for 0% -> 0%
where the time goes in v1:
time: 630 us; the launch traced here: 629 us
  waiting for transfers between devices  531 us (84%)
  matrix products  36.2 us (6%)
  other arithmetic  19.8 us (3%)
  Pallas kernels  15.1 us (2%)
  between operations  13.6 us (2%)
  local copies, waits for them, and re-layouts  13.5 us (2%)
    reduce_scatter x1, waiting for transfers between devices, on_device(): lax.psum_scatter(head_term.astype(jnp.bfloat16), 'tp', scatter_dimension=...  103 us
    all_gather x1, waiting for transfers between devices, on_device(): lax.all_gather(w_down, 'sp', axis=0, tiled=True)  92.6 us
    all_gather x1, waiting for transfers between devices, on_device(): lax.all_gather(w_gate, 'sp', axis=0, tiled=True)  88.9 us
    all_gather x1, waiting for transfers between devices, on_device(): latent_all = lax.all_gather(packed, 'sp', axis=0, tiled=True)  85.3 us
    all_gather x1, waiting for transfers between devices, on_device(): lax.all_gather(w_up, 'sp', axis=0, tiled=True)  82.7 us
    reduce_scatter x1, waiting for transfers between devices, on_device(): lax.psum_scatter(down_term.astype(jnp.bfloat16), 'tp', scatter_dimension=...  42.9 us
    all_gather x1, waiting for transfers between devices, on_device(): row_piece = lax.all_gather(normed, 'tp', axis=0, tiled=True)  34.1 us
    dot_general x1, matrix products, on_device(): lax.dot_general(hidden, down_full, COLS, preferred_element_type=jnp.float32)  20.6 us
  transfers between devices with their start and end apart: 7, of which 7 were waited for; matrix products, arithmetic and copies ran while one was open for 5% of the time, Pallas kernels for 0%

profile of v1, /device:TPU:0, one launch (start us, length us, event | category | flops | bytes accessed | tf_op | source)
XLA Modules:
  0.0 629.4 jit_solution(7614648743395461173)
XLA Ops:
  6.5 1.2 copy.31
  7.8 1.3 fusion
  9.1 0.1 pad.3.clone
  9.2 1.2 fusion.2
  10.5 3.2 subtract_convert_fusion.1
  13.7 1.2 maximum_maximum_fusion
  14.8 0.0 all-gather.6.cloned.1.call-update
  14.8 0.0 reduce-scatter.3.cloned.1.call-start
  14.9 0.1 pad.7.clone
  15.0 0.2 copy.26
  15.2 0.9 fusion.3
  16.1 3.0 copy.36
  19.1 2.0 copy.37
  21.1 1.5 copy.25
  22.6 1.3 copy.30
  23.9 0.1 copy.32
  24.0 0.2 copy.33
  24.2 1.1 copy.34
  25.3 0.2 copy.35
  25.5 0.0 copy-start.4
  25.5 3.4 subtract_convert_fusion
  29.0 2.1 maximum_bitcast_fusion.q_ref
  31.1 85.3 %all-gather.6.cloned.1.call-done.lat_ref = bf16[8192,384]{1,0:T(8,128)(2,1)} async-done(((bf16[1024,384]{1,0:T(8,128)(2,1)}), bf16[8192,384]{1,0:T(8,128)(2,1)}) %all-gather.6.cloned.1.call-update) | async-done | bytes 6291472 | tf_op jit(solution)/shard_map/all_gather | solution.py:172
  116.4 1.6 copy-done.2
  118.0 15.1 %shard_map.127 = bf16[4,1024,128]{2,1,0:T(8,128)(2,1)S(1)} custom-call(bf16[4,1024,256]{2,1,0:T(8,128)(2,1)S(1)} %copy-done.2, bf16[8192,384]{1,0:T(8,128)(2,1)} %all-gather.6.cloned.1.call-done.lat_ref, bf16[4,256,128]{2,1,0:T(8,128)(2,1)S(1)} %bitcast.29, bf16[4,256,128]{2,1,0:T(8,128)(2,1)S(1)} %bitcast.30), custom_call_target="tpu_custom_call" | custom-call | flops 34359738368 | bytes 8388608 | tf_op jit(solution)/shard_map/pallas_call | solution.py:119
  133.1 3.9 bitcast_convert_fusion
  137.0 0.0 reduce-scatter.3.cloned.1.call-update
  137.0 0.0 all-gather.10.cloned.1.call-start
  137.1 0.7 all-gather.10.cloned.1.call-update
  137.8 0.0 all-gather.8.cloned.1.call-start
  137.8 102.6 %reduce-scatter.3.cloned.1.call-done = bf16[256,2048]{1,0:T(8,128)(2,1)} async-done(((bf16[1024,2048]{1,0:T(8,128)(2,1)}), bf16[256,2048]{1,0:T(8,128)(2,1)}) %reduce-scatter.3.cloned.1.call-update) | async-done | bytes 1048592 | tf_op jit(solution)/shard_map/reduce_scatter | solution.py:194
  240.4 1.6 multiply_reduce_fusion
  242.1 2.6 multiply_convert_fusion.1
  244.7 0.0 all-gather.8.cloned.1.call-update
  244.7 0.0 all-gather.12.cloned.1.call-start
  244.7 0.5 all-gather.12.cloned.1.call-update
  245.3 0.0 all-gather.14.cloned.1.call-start
  245.3 0.5 all-gather.14.cloned.1.call-update
  245.8 0.2 reduce-scatter.5.cloned.1.call-start
  246.1 88.9 %all-gather.10.cloned.1.call-done = bf16[2048,1408]{1,0:T(8,128)(2,1)} async-done(((bf16[256,1408]{1,0:T(8,128)(2,1)}), bf16[2048,1408]{1,0:T(8,128)(2,1)}) %all-gather.10.cloned.1.call-update) | async-done | bytes 5767184 | tf_op jit(solution)/shard_map/all_gather | solution.py:174
  335.0 34.1 %all-gather.8.cloned.1.call-done = bf16[1024,2048]{1,0:T(8,128)(2,1)} async-done(((bf16[256,2048]{1,0:T(8,128)(2,1)}), bf16[1024,2048]{1,0:T(8,128)(2,1)}) %all-gather.8.cloned.1.call-update) | async-done | bytes 4194320 | tf_op jit(solution)/shard_map/all_gather | solution.py:199
  369.0 11.7 %fusion.4 = f32[1024,1408]{1,0:T(8,128)} fusion(bf16[1024,2048]{1,0:T(8,128)(2,1)} %all-gather.8.cloned.1.call-done, bf16[2048,1408]{1,0:T(8,128)(2,1)} %all-gather.10.cloned.1.call-done), kind=kOutput, calls=%fused_computation.25 | convolution fusion | flops 5905580032 | bytes 15728640 | tf_op jit(solution)/shard_map/dot_general | solution.py:200
  380.7 82.7 %all-gather.12.cloned.1.call-done = bf16[2048,1408]{1,0:T(8,128)(2,1)} async-done(((bf16[256,1408]{1,0:T(8,128)(2,1)}), bf16[2048,1408]{1,0:T(8,128)(2,1)}) %all-gather.12.cloned.1.call-update) | async-done | bytes 5767184 | tf_op jit(solution)/shard_map/all_gather | solution.py:175
  463.4 92.6 %all-gather.14.cloned.1.call-done = bf16[2048,1408]{1,0:T(8,128)(2,1)} async-done(((bf16[256,1408]{1,0:T(8,128)(2,1)}), bf16[2048,1408]{1,0:T(8,128)(2,1)}) %all-gather.14.cloned.1.call-update) | async-done | bytes 5767184 | tf_op jit(solution)/shard_map/all_gather | solution.py:176
  556.0 20.6 %convolution_convert_fusion = bf16[1024,2048]{1,0:T(8,128)(2,1)} fusion(bf16[2048,1408]{1,0:T(8,128)(2,1)} %all-gather.14.cloned.1.call-done, f32[1024,1408]{1,0:T(8,128)} %fusion.4, bf16[1024,2048]{1,0:T(8,128)(2,1)} %all-gather.8.cloned.1.call-done, bf16[2048,1408]{1,0:T(8,128)(2,1)} %all-gather.12.cloned.1.call-done), kind=kOutput, calls=%fused_computation.2 | convolution fusion | flops 11821907968 | bytes 25690112 | tf_op jit(solution)/shard_map/dot_general | solution.py:203
  576.6 0.0 reduce-scatter.5.cloned.1.call-update
  576.6 42.9 %reduce-scatter.5.cloned.1.call-done = bf16[256,2048]{1,0:T(8,128)(2,1)} async-done(((bf16[1024,2048]{1,0:T(8,128)(2,1)}), bf16[256,2048]{1,0:T(8,128)(2,1)}) %reduce-scatter.5.cloned.1.call-update) | async-done | bytes 1048592 | tf_op jit(solution)/shard_map/reduce_scatter | solution.py:204
  619.5 3.1 add_convert_fusion
  (21 shorter events, 0.1 us)
Async XLA Ops:
  6.5 126.5 %copy-start = (bf16[512,2048]{1,0:T(8,128)(2,1)S(1)}, bf16[512,2048]{1,0:T(8,128)(2,1)}, u32[]{:S(2)}) copy-start(bf16[512,2048]{1,0:T(8,128)(2,1)} %param.21) | copy-start | bytes 6291460
  6.5 109.9 %all-gather.6.cloned.1.call-start = ((), (), s32[]{:S(2)}) async-start(), calls=%async_computation.2 | async-start | bytes 7077888 | tf_op jit(solution)/shard_map/all_gather | solution.py:172
  10.4 4.5 copy-start.5
  14.8 225.6 %reduce-scatter.3.cloned.1.call-start = ((), (), s32[]{:S(2)}) async-start(), calls=%async_computation.3 | async-start | bytes 5242880 | tf_op jit(solution)/shard_map/reduce_scatter | solution.py:194
  19.1 4.8 copy-start.6
  25.5 3.5 copy-start.4
  116.4 1.6 copy-start.2
  137.0 103.4 %copy-start.3 = (bf16[256,2048]{1,0:T(8,128)(2,1)S(1)}, bf16[256,2048]{1,0:T(8,128)(2,1)}, u32[]{:S(2)}) copy-start(bf16[256,2048]{1,0:T(8,128)(2,1)} %param.13) | copy-start | bytes 3145732
  137.0 105.1 %copy-start.7 = (f32[2048]{0:T(1024)S(1)}, f32[2048]{0:T(1024)}, u32[]{:S(2)}) copy-start(f32[2048]{0:T(1024)} %param.22) | copy-start | bytes 24580
  137.0 197.9 %all-gather.10.cloned.1.call-start = ((), (), s32[]{:S(2)}) async-start(), calls=%async_computation.5 | async-start | bytes 6488064 | tf_op jit(solution)/shard_map/all_gather | solution.py:174
  137.8 231.3 %all-gather.8.cloned.1.call-start = ((), (), s32[]{:S(2)}) async-start(), calls=%async_computation.4 | async-start | bytes 5242880 | tf_op jit(solution)/shard_map/all_gather | solution.py:199
  244.7 218.7 %all-gather.12.cloned.1.call-start = ((), (), s32[]{:S(2)}) async-start(), calls=%async_computation.6 | async-start | bytes 6488064 | tf_op jit(solution)/shard_map/all_gather | solution.py:175
  245.3 310.7 %all-gather.14.cloned.1.call-start = ((), (), s32[]{:S(2)}) async-start(), calls=%async_computation.7 | async-start | bytes 6488064 | tf_op jit(solution)/shard_map/all_gather | solution.py:176
  245.8 373.7 %reduce-scatter.5.cloned.1.call-start = ((), (), s32[]{:S(2)}) async-start(), calls=%async_computation.8 | async-start | bytes 5242880 | tf_op jit(solution)/shard_map/reduce_scatter | solution.py:204
  576.6 46.0 %copy-start.1 = (bf16[512,2048]{1,0:T(8,128)(2,1)S(1)}, bf16[512,2048]{1,0:T(8,128)(2,1)}, u32[]{:S(2)}) copy-start(bf16[512,2048]{1,0:T(8,128)(2,1)} %param.21) | copy-start | bytes 6291460
Sparse Core Ops, SparseCore 0:
  15.0 101.4 all-gather.5
  137.1 103.2 reduce-scatter.2
  242.6 92.3 all-gather.9
  336.4 32.6 all-gather.7
  371.1 92.3 all-gather.11
  465.5 90.4 all-gather.13
  576.7 42.7 reduce-scatter.4
